TPU v7x, 32 devices: a whole 2x2x4 slice. The times are simulated.
32 devices in a mesh: ep: 8 (over z, x), tp: 4 (over y, core).
Axes of the slice: x: 2, y: 2, z: 4, core: 2. Of those that a mesh axis runs over, the one named last changes fastest.
Arguments:
- mixer_input: bfloat16 [5120, 2048], P('ep'), may hold values from -6 to 6
- mixer_gain: float32 [2048], replicated, may hold values from 0.1 to 1.9
- value_weight: bfloat16 [2048, 1024], P(None, 'tp'), may hold values from -0.125 to 0.125
- inner_gate: bfloat16 [2048, 1024], P(None, 'tp'), may hold values from -0.125 to 0.125
- outer_gate: bfloat16 [2048, 1024], P(None, 'tp'), may hold values from -0.125 to 0.125
- kernel_taps: float32 [3, 1024], P(None, 'tp'), may hold values from -3 to 3
- mixer_proj: bfloat16 [1024, 2048], P('tp'), may hold values from -0.1875 to 0.1875
- expert_input: bfloat16 [5120, 2048], P(('ep', 'tp')), may hold values from -6 to 6
- expert_gain: float32 [2048], replicated, may hold values from 0.1 to 1.9
- routes: int32 [5120, 2], P(('ep', 'tp')), may hold values from 0 to 7, as said below
- group_logits: float32 [5120, 1], P(('ep', 'tp')), may hold values from -6 to 6
- pair_logits: float32 [5120, 2], P(('ep', 'tp')), may hold values from -6 to 6
- gate_weight: bfloat16 [8, 2048, 1024], P('ep', None, 'tp'), may hold values from -0.125 to 0.125
- up_weight: bfloat16 [8, 2048, 1024], P('ep', None, 'tp'), may hold values from -0.125 to 0.125
- down_weight: bfloat16 [8, 1024, 2048], P('ep', 'tp'), may hold values from -0.75 to 0.75
Outputs:
- mixer_output: bfloat16 [5120, 2048], P(('ep', 'tp'))
- expert_output: bfloat16 [5120, 2048], P(('ep', 'tp'))
Inputs may be any that keep to these rules, and one draw needn't show every extreme that they name: `routes`: both entries of a row are different experts of one group (equal after integer division by 8). In the rows of one device every group is chosen by the same number of rows, no expert is named more than 80 times, and in every draw one expert is named exactly 80 times in the rows of every device.
All inputs are finite; a program needn't handle non-finite values.
Results may differ from a plain program's by a relative error of at most 0.01.
Values may be sent and summed in bfloat16 or wider, within the bound.
A program may use at most 128 MiB of HBM per device.

v0:
```python
import jax
import jax.numpy as jnp
from jax import lax
from jax.sharding import PartitionSpec as P

EPG = 8
EPSILON = 1e-06


def padded_2(cells, sides, width):
    for axis, dim in sides:
        count = lax.axis_size(axis)
        ends = count - 1
        head = lax.slice_in_dim(cells, 0, width, axis=dim)
        tail = lax.slice_in_dim(cells, cells.shape[dim] - width, cells.shape[dim], axis=dim)
        cells = jnp.concatenate(
            [
                lax.ppermute(tail, axis, [(i, (i + 1) % count) for i in range(ends)]),
                cells,
                lax.ppermute(head, axis, [((i + 1) % count, i) for i in range(ends)]),
            ],
            axis=dim,
        )
    return cells


def normed(values, gain):
    wide = values.astype(jnp.float32)
    scale = lax.rsqrt(jnp.mean(wide * wide, axis=-1, keepdims=True) + EPSILON)
    return (wide * scale * gain).astype(jnp.bfloat16)


def blockwise_sum(left, right, blocks):
    width = left.shape[1] // blocks
    total = jnp.zeros((left.shape[0], right.shape[1]), jnp.float32)
    for block in range(blocks):
        part = jnp.dot(
            left[:, block * width : (block + 1) * width],
            right[block * width : (block + 1) * width],
            preferred_element_type=jnp.float32,
        )
        rounded = lax.optimization_barrier(part.astype(jnp.bfloat16))
        total = total + rounded.astype(jnp.float32)
    return total.astype(jnp.bfloat16)


def route_weights(routes, group_logits, pair_logits):
    chosen = routes[:, 0] // EPG
    groups = jnp.arange(group_logits.shape[1], dtype=jnp.int32)
    picked = jnp.sum(jnp.where(groups[None, :] == chosen[:, None], group_logits, 0.0), axis=1)
    group_weight = 1.0 / jnp.sum(jnp.exp(group_logits - picked[:, None]), axis=1)
    return group_weight[:, None] * jax.nn.sigmoid(pair_logits - pair_logits[:, ::-1])


def on_device(
    mixer_input,
    mixer_gain,
    value_weight,
    inner_gate,
    outer_gate,
    kernel_taps,
    mixer_proj,
    expert_input,
    expert_gain,
    routes,
    group_logits,
    pair_logits,
    gate_weight,
    up_weight,
    down_weight,
):
    split = lax.axis_size("tp")
    normal_rows = normed(mixer_input, mixer_gain)
    values = jnp.dot(normal_rows, value_weight, preferred_element_type=jnp.float32)
    inner = jnp.dot(normal_rows, inner_gate, preferred_element_type=jnp.float32)
    outer = jnp.dot(normal_rows, outer_gate, preferred_element_type=jnp.float32)
    mixed_in = (inner * values).astype(jnp.bfloat16)
    padded = padded_2(mixed_in, (("ep", 0),), 1).astype(jnp.float32)
    conv_sum = (
        kernel_taps[0] * padded[:-2] + kernel_taps[1] * padded[1:-1] + kernel_taps[2] * padded[2:]
    )
    mixer_rows = (outer * conv_sum).astype(jnp.bfloat16)
    mixer_output = lax.psum_scatter(
        jnp.dot(mixer_rows, mixer_proj, preferred_element_type=jnp.float32).astype(jnp.bfloat16),
        "tp",
        scatter_dimension=0,
        tiled=True,
    )
    expert_norm = normed(expert_input, expert_gain)
    weights = route_weights(routes, group_logits, pair_logits)
    experts = lax.axis_size("ep")
    local = expert_norm.shape[0]
    width = expert_norm.shape[1]
    capacity = 4 * local // experts
    flat = routes.reshape(-1)
    onehot = (flat[:, None] == jnp.arange(experts, dtype=jnp.int32)[None, :]).astype(jnp.int32)
    before = jnp.sum((jnp.cumsum(onehot, axis=0) - onehot) * onehot, axis=1)
    slots = flat * capacity + before
    sources = (
        jnp.full((experts * capacity,), local, jnp.int32)
        .at[slots]
        .set(jnp.arange(2 * local, dtype=jnp.int32) // 2)
    )
    rows_pad = jnp.concatenate([expert_norm, jnp.zeros((1, width), jnp.bfloat16)])
    outgoing = rows_pad[sources].reshape(experts, capacity, width)
    whole_gate, whole_up, whole_down = (
        lax.all_gather(gate_weight, "tp", axis=2, tiled=True),
        lax.all_gather(up_weight, "tp", axis=2, tiled=True),
        lax.all_gather(down_weight, "tp", axis=1, tiled=True),
    )
    arrived = lax.all_to_all(outgoing, "ep", split_axis=0, concat_axis=0, tiled=True)
    senders, items, _ = arrived.shape
    answers = expert_block_local(
        arrived.reshape(senders * items, width), whole_gate[0], whole_up[0], whole_down[0], split
    )
    returned = lax.all_to_all(
        answers.reshape(senders, items, width), "ep", split_axis=0, concat_axis=0, tiled=True
    )
    answered = returned.reshape(experts * capacity, width)
    pairs = answered[slots].reshape(local, 2, width)
    expert_output = (
        weights[:, 0:1] * pairs[:, 0].astype(jnp.float32)
        + weights[:, 1:2] * pairs[:, 1].astype(jnp.float32)
    ).astype(jnp.bfloat16)
    return (mixer_output, expert_output)


def expert_block_local(rows, gate, upper, down, blocks):
    first = jnp.dot(rows, gate, preferred_element_type=jnp.float32)
    second = jnp.dot(rows, upper, preferred_element_type=jnp.float32)
    hidden = (jax.nn.silu(first) * second).astype(jnp.bfloat16)
    return blockwise_sum(hidden, down, blocks)


def solution(mesh):
    in_specs = (
        P("ep", None),
        P(),
        P(None, "tp"),
        P(None, "tp"),
        P(None, "tp"),
        P(None, "tp"),
        P("tp", None),
        P(("ep", "tp"), None),
        P(),
        P(("ep", "tp"), None),
        P(("ep", "tp"), None),
        P(("ep", "tp"), None),
        P("ep", None, "tp"),
        P("ep", None, "tp"),
        P("ep", "tp", None),
    )
    out_specs = (P(("ep", "tp"), None), P(("ep", "tp"), None))
    return jax.shard_map(
        on_device, mesh=mesh, in_specs=in_specs, out_specs=out_specs, check_vma=False
    )
```

profile of v0, /device:TPU:0, one launch (start us, length us, event | category | flops | bytes accessed | tf_op | source)
XLA Modules:
  0.0 216.1 jit_solution(17580793458356525415)
XLA Ops:
  7.2 0.0 copy-start
  7.2 0.0 copy-start.3
  7.2 0.0 copy-start.5
  7.2 0.0 all-gather.6.cloned.1.call-start
  7.2 0.7 all-gather.6.cloned.1.call-update
  7.9 0.0 all-gather.4.cloned.1.call-start
  8.0 0.7 all-gather.4.cloned.1.call-update
  8.7 0.8 copy.20
  9.5 0.1 eq.29
  9.6 0.9 reduce-window.6
  10.5 0.2 slice_reduce_fusion
  10.8 0.7 broadcast_multiply_fusion
  11.5 0.1 copy.19
  11.6 0.1 mul.158
  11.7 0.0 copy-done.3
  11.7 0.2 fusion.9
  12.0 0.0 copy-done.5
  12.0 0.2 fusion.11
  12.2 0.1 concatenate.7
  12.3 0.1 add_bitcast_fusion
  12.4 2.9 %scatter_custom_fusion = s32[640]{0:T(1024)S(1)} fusion(s32[320]{0:T(512)S(1)} %fusion.34, s32[320]{0:T(512)S(1)} %add_select_fusion, s32[]{:T(128)} %constant.59.clone.1), kind=kCustom, calls=%fused_computation.75 | custom fusion | bytes 2564 | tf_op jit(solution)/shard_map/scatter | solution.py:102
  15.3 4.1 %gather_fusion = bf16[640,2048]{1,0:T(8,128)(2,1)} fusion(bf16[161,2048]{1,0:T(8,128)(2,1)S(1)} %concatenate.7, s32[1024]{0:T(1024)S(1)} %pad_clamp_fusion.1), kind=kCustom, calls=%fused_computation | custom fusion | bytes 5245440 | tf_op jit(solution)/shard_map/gather | solution.py:105
  19.4 7.3 %all-to-all-start = ((bf16[8,80,2048]{2,1,0:T(8,128)(2,1)}), bf16[8,80,2048]{2,1,0:T(8,128)(2,1)}, u32[]{:S(2)}, u32[]{:S(2)}) async-start(bf16[8,80,2048]{2,1,0:T(8,128)(2,1)} %bitcast.53), calls=%async_computation.1 | async-start | bytes 5242880 | tf_op jit(solution)/shard_map/all_to_all | solution.py:111
  26.7 0.0 copy-start.12
  26.7 0.0 all-gather.8.cloned.1.call-start
  26.7 0.7 all-gather.8.cloned.1.call-update
  27.4 0.0 copy-start.2
  27.4 2.5 %fusion = f32[640]{0:T(1024)S(1)} fusion(bf16[640,2048]{1,0:T(8,128)(2,1)} %param.15), kind=kLoop, calls=%fused_computation.5 | loop fusion | flops 3931520 | bytes 2624000 | tf_op jit(solution)/shard_map/reduce_sum | solution.py:29
  29.9 0.0 copy-done.9
  29.9 0.0 copy-done.12
  29.9 0.1 copy-done.2
  30.0 0.9 fusion.37
  31.0 0.3 copy-done.10
  31.3 0.9 fusion.15
  32.2 3.9 %collective-permute-start = (bf16[1,256]{1,0:T(2,128)(2,1)S(1)}, bf16[1,256]{1,0:T(2,128)(2,1)S(1)}, u32[]{:S(2)}, u32[]{:S(2)}) collective-permute-start(bf16[1,256]{1,0:T(2,128)(2,1)S(1)} %get-tuple-element.4), channel_id=1, source_target_pairs={{0,4},{4,8},{8,12},{12,16},{16,20},{20,24},{24,28},{1,5},{5,9},{9,... | collective-permute-start | bytes 1544 | tf_op jit(solution)/shard_map/ppermute | solution.py:18
  36.1 1.5 collective-permute-start.1
  37.6 0.0 copy-done.7
  37.6 10.4 %collective-permute-done = bf16[1,256]{1,0:T(2,128)(2,1)S(1)} collective-permute-done((bf16[1,256]{1,0:T(2,128)(2,1)S(1)}, bf16[1,256]{1,0:T(2,128)(2,1)S(1)}, u32[]{:S(2)}, u32[]{:S(2)}) %collective-permute-start) | collective-permute-done | bytes 544 | tf_op jit(solution)/shard_map/ppermute | solution.py:18
  48.1 0.0 collective-permute-done.1
  48.1 0.1 maximum_convert_fusion
  48.2 38.1 %all-to-all-done = bf16[8,80,2048]{2,1,0:T(8,128)(2,1)} async-done(((bf16[8,80,2048]{2,1,0:T(8,128)(2,1)}), bf16[8,80,2048]{2,1,0:T(8,128)(2,1)}, u32[]{:S(2)}, u32[]{:S(2)}) %all-to-all-start) | async-done | bytes 2621472 | tf_op jit(solution)/shard_map/all_to_all | solution.py:111
  86.3 7.3 %fusion.3 = f32[640,1024]{1,0:T(8,128)} fusion(bf16[640,2048]{1,0:T(8,128)(2,1)} %bitcast.9, bf16[1,2048,1024]{2,1,0:T(8,128)(2,1)} %all-gather.6.cloned.1.call-done), kind=kOutput, calls=%fused_computation.9 | convolution fusion | flops 2684354560 | bytes 9437184 | tf_op jit(solution)/shard_map/dot_general | solution.py:130
  93.6 7.5 %multiply_convert_fusion = bf16[640,1024]{1,0:T(8,128)(2,1)S(1)} fusion(f32[640,1024]{1,0:T(8,128)} %fusion.3, bf16[640,2048]{1,0:T(8,128)(2,1)} %bitcast.9, bf16[1,2048,1024]{2,1,0:T(8,128)(2,1)} %all-gather.4.cloned.1.call-done), kind=kOutput, calls=%fused_computation.18 | convolution fusion | flops 2688286720 | bytes 10747904 | tf_op jit(solution)/shard_map/dot_general | solution.py:129
  101.1 18.9 %all-gather.8.cloned.1.call-done = bf16[1,1024,2048]{2,1,0:T(8,128)(2,1)} async-done(((bf16[1,256,2048]{2,1,0:T(8,128)(2,1)}), bf16[1,1024,2048]{2,1,0:T(8,128)(2,1)}) %all-gather.8.cloned.1.call-update) | async-done | bytes 4194320 | tf_op jit(solution)/shard_map/all_gather | solution.py:109
  120.0 2.2 %convolution_convert_fusion.3 = bf16[640,2048]{1,0:T(8,128)(2,1)S(1)} fusion(bf16[1,1024,2048]{2,1,0:T(8,128)(2,1)} %all-gather.8.cloned.1.call-done, bf16[640,1024]{1,0:T(8,128)(2,1)S(1)} %multiply_convert_fusion), kind=kOutput, calls=%fused_computation.16 | convolution fusion | flops 672399360 | bytes 3997696 | tf_op jit(solution)/shard_map/dot_general | solution.py:37
  122.2 2.1 convolution_convert_fusion.2
  124.3 0.0 copy-done.1
  124.3 0.9 convolution_convert_fusion.1
  125.2 0.9 convolution_convert_fusion
  126.0 3.8 %add_convert_fusion = bf16[640,2048]{1,0:T(8,128)(2,1)} fusion(bf16[640,2048]{1,0:T(8,128)(2,1)S(1)} %convolution_convert_fusion, bf16[640,2048]{1,0:T(8,128)(2,1)S(1)} %convolution_convert_fusion.1, bf16[640,2048]{1,0:T(8,128)(2,1)S(1)} %convolution_convert_fusion.2, bf16[640,2048]{1,0:T(8,128)(2,1)S(1)} %convolution_convert_fusion.3), kind=kLoop, calls=%fused_computation.8 | loop fusion | flops 10485760 | bytes 13107200 | tf_op jit(solution)/shard_map/convert_element_type | solution.py:44
  129.9 5.6 %all-to-all-start.1 = ((bf16[8,80,2048]{2,1,0:T(8,128)(2,1)}), bf16[8,80,2048]{2,1,0:T(8,128)(2,1)}, u32[]{:S(2)}, u32[]{:S(2)}) async-start(bf16[8,80,2048]{2,1,0:T(8,128)(2,1)} %bitcast.54), calls=%async_computation.2 | async-start | bytes 5242880 | tf_op jit(solution)/shard_map/all_to_all | solution.py:116
  135.5 0.3 reduce-scatter.2.cloned.1.call-start
  135.8 0.0 copy-done
  135.8 0.0 copy-done.11
  135.8 6.1 %convolution_convert_fusion.4 = bf16[640,2048]{1,0:T(8,128)(2,1)} fusion(bf16[256,2048]{1,0:T(8,128)(2,1)S(1)} %copy-done, bf16[2048,256]{1,0:T(8,128)(2,1)S(1)} %copy-done.11, f32[642,256]{1,0:T(8,128)S(1)} %maximum_convert_fusion, f32[256]{0:T(256)S(1)} %bitcast.60, f32[256]{0:T(256)S(1)} %bitcast.61, f32[256]{0:T(256)S(1)} %bitcast.59, ...), kind=kOutput, calls=%fused_computation.17 | convolution fusion | flops 1349877760 | bytes 9321472 | tf_op jit(solution)/shard_map/dot_general | solution.py:84
  141.9 0.0 reduce-scatter.2.cloned.1.call-update
  141.9 0.7 copy-done.6
  142.7 0.0 copy-done.4
  142.7 0.0 copy-done.8
  142.7 52.8 %all-to-all-done.1 = bf16[8,80,2048]{2,1,0:T(8,128)(2,1)} async-done(((bf16[8,80,2048]{2,1,0:T(8,128)(2,1)}), bf16[8,80,2048]{2,1,0:T(8,128)(2,1)}, u32[]{:S(2)}, u32[]{:S(2)}) %all-to-all-start.1) | async-done | bytes 2621472 | tf_op jit(solution)/shard_map/all_to_all | solution.py:116
  195.5 7.0 %gather_fusion.1 = bf16[320,2048]{1,0:T(8,128)(2,1)} fusion(bf16[640,2048]{1,0:T(8,128)(2,1)} %bitcast.17, s32[1024]{0:T(1024)S(1)} %pad_clamp_fusion), kind=kCustom, calls=%fused_computation.1 | custom fusion | bytes 2622720 | tf_op jit(solution)/shard_map/gather | solution.py:120
  202.5 3.1 %reshape.96 = bf16[160,2,2048]{2,1,0:T(2,128)(2,1)S(1)} reshape(bf16[320,2048]{1,0:T(8,128)(2,1)} %gather_fusion.1) | data formatting | bytes 2621440 | tf_op jit(solution)/shard_map/reshape | solution.py:120
  205.6 1.8 fusion.41
  207.4 2.2 %fusion.13 = bf16[160,2048]{1,0:T(8,128)(2,1)} fusion(bf16[160,1,2048]{2,1,0:T(2,128)(2,1)S(1)} %get-tuple-element.3, bf16[160,1,2048]{2,1,0:T(2,128)(2,1)S(1)} %get-tuple-element.2, f32[160]{0:T(256)S(1)} %bitcast.57, f32[160]{0:T(256)S(1)} %bitcast.56), kind=kLoop, calls=%fused_computation.26 | loop fusion | flops 1966080 | bytes 1967360 | tf_op jit(solution)/shard_map/convert_element_type | solution.py:124
  (28 shorter events, 0.2 us)
Async XLA Ops:
  7.2 128.6 %copy-start = (bf16[256,2048]{1,0:T(8,128)(2,1)S(1)}, bf16[256,2048]{1,0:T(8,128)(2,1)}, u32[]{:S(2)}) copy-start(bf16[256,2048]{1,0:T(8,128)(2,1)} %param.21) | copy-start | bytes 3145732
  7.2 4.5 %copy-start.3 = (bf16[160,2048]{1,0:T(8,128)(2,1)S(1)}, bf16[160,2048]{1,0:T(8,128)(2,1)}, u32[]{:S(2)}) copy-start(bf16[160,2048]{1,0:T(8,128)(2,1)} %param.22) | copy-start | bytes 1966084
  7.2 4.8 %copy-start.5 = (f32[2048]{0:T(1024)S(1)}, f32[2048]{0:T(1024)}, u32[]{:S(2)}) copy-start(f32[2048]{0:T(1024)} %param.23) | copy-start | bytes 24580
  7.2 79.1 %all-gather.6.cloned.1.call-start = ((), (), s32[]{:S(2)}) async-start(), calls=%async_computation.5 | async-start | bytes 5242880 | tf_op jit(solution)/shard_map/all_gather | solution.py:108
  7.9 85.6 %all-gather.4.cloned.1.call-start = ((), (), s32[]{:S(2)}) async-start(), calls=%async_computation.4 | async-start | bytes 5242880 | tf_op jit(solution)/shard_map/all_gather | solution.py:107
  19.4 66.9 %all-to-all-start = ((bf16[8,80,2048]{2,1,0:T(8,128)(2,1)}), bf16[8,80,2048]{2,1,0:T(8,128)(2,1)}, u32[]{:S(2)}, u32[]{:S(2)}) async-start(bf16[8,80,2048]{2,1,0:T(8,128)(2,1)} %bitcast.53), calls=%async_computation.1 | async-start | bytes 5242880 | tf_op jit(solution)/shard_map/all_to_all | solution.py:111
  26.7 3.2 %copy-start.9 = (bf16[2048,256]{1,0:T(8,128)(2,1)S(1)}, bf16[2048,256]{1,0:T(8,128)(2,1)}, u32[]{:S(2)}) copy-start(bf16[2048,256]{1,0:T(8,128)(2,1)} %param.18) | copy-start | bytes 3145732
  26.7 3.3 %copy-start.12 = (f32[2048]{0:T(1024)S(1)}, f32[2048]{0:T(1024)}, u32[]{:S(2)}) copy-start(f32[2048]{0:T(1024)} %param.16) | copy-start | bytes 24580
  26.7 93.3 %all-gather.8.cloned.1.call-start = ((), (), s32[]{:S(2)}) async-start(), calls=%async_computation.6 | async-start | bytes 5242880 | tf_op jit(solution)/shard_map/all_gather | solution.py:109
  27.4 2.6 %copy-start.2 = (bf16[640,2048]{1,0:T(8,128)(2,1)S(1)}, bf16[640,2048]{1,0:T(8,128)(2,1)}, u32[]{:S(2)}) copy-start(bf16[640,2048]{1,0:T(8,128)(2,1)} %param.15) | copy-start | bytes 7864324
  30.0 1.2 copy-start.10
  31.3 6.3 %copy-start.7 = (f32[3,256]{1,0:T(4,128)S(1)}, f32[3,256]{1,0:T(4,128)}, u32[]{:S(2)}) copy-start(f32[3,256]{1,0:T(4,128)} %param.20) | copy-start | bytes 9220
  32.2 15.9 %collective-permute-start = (bf16[1,256]{1,0:T(2,128)(2,1)S(1)}, bf16[1,256]{1,0:T(2,128)(2,1)S(1)}, u32[]{:S(2)}, u32[]{:S(2)}) collective-permute-start(bf16[1,256]{1,0:T(2,128)(2,1)S(1)} %get-tuple-element.4), channel_id=1, source_target_pairs={{0,4},{4,8},{8,12},{12,16},{16,20},{20,24},{24,28},{1,5},{5,9},{9,... | collective-permute-start | bytes 1544 | tf_op jit(solution)/shard_map/ppermute | solution.py:18
  36.1 11.9 %collective-permute-start.1 = (bf16[1,256]{1,0:T(2,128)(2,1)S(1)}, bf16[1,256]{1,0:T(2,128)(2,1)S(1)}, u32[]{:S(2)}, u32[]{:S(2)}) collective-permute-start(bf16[1,256]{1,0:T(2,128)(2,1)S(1)} %get-tuple-element.5), channel_id=1, source_target_pairs={{4,0},{8,4},{12,8},{16,12},{20,16},{24,20},{28,24},{5,1},{9,5},{13... | collective-permute-start | bytes 1544 | tf_op jit(solution)/shard_map/ppermute | solution.py:20
  120.0 4.3 %copy-start.1 = (bf16[1,1024,2048]{2,1,0:T(8,128)(2,1)S(1)}, bf16[1,1024,2048]{2,1,0:T(8,128)(2,1)}, u32[]{:S(2)}) copy-start(bf16[1,1024,2048]{2,1,0:T(8,128)(2,1)} %all-gather.8.cloned.1.call-done) | copy-start | bytes 12582916
  129.9 5.9 %copy-start.11 = (bf16[2048,256]{1,0:T(8,128)(2,1)S(1)}, bf16[2048,256]{1,0:T(8,128)(2,1)}, u32[]{:S(2)}) copy-start(bf16[2048,256]{1,0:T(8,128)(2,1)} %param.19) | copy-start | bytes 3145732
  129.9 65.6 %all-to-all-start.1 = ((bf16[8,80,2048]{2,1,0:T(8,128)(2,1)}), bf16[8,80,2048]{2,1,0:T(8,128)(2,1)}, u32[]{:S(2)}, u32[]{:S(2)}) async-start(bf16[8,80,2048]{2,1,0:T(8,128)(2,1)} %bitcast.54), calls=%async_computation.2 | async-start | bytes 5242880 | tf_op jit(solution)/shard_map/all_to_all | solution.py:116
  135.5 74.1 %reduce-scatter.2.cloned.1.call-start = ((), (), s32[]{:S(2)}) async-start(), calls=%async_computation.3 | async-start | bytes 3276800 | tf_op jit(solution)/shard_map/reduce_scatter | solution.py:83
  141.9 0.7 copy-start.6
  141.9 0.8 copy-start.4
  141.9 0.8 copy-start.8
Sparse Core Ops, SparseCore 0:
  9.6 37.7 all-gather.5
  48.9 34.9 all-gather.3
  85.5 34.4 all-gather.7
  142.1 34.7 reduce-scatter.1
where the time goes:
time: 217 us; the launch traced here: 216 us
  waiting for transfers between devices  122 us (56%)
  matrix products  28.8 us (13%)
  local copies, waits for them, and re-layouts  21.5 us (10%)
  starting transfers between devices  18.7 us (9%)
  between operations  14.1 us (6%)
  other arithmetic  10.8 us (5%)
    all_to_all x1, waiting for transfers between devices, on_device(): lax.all_to_all(answers.reshape(senders, items, width), 'ep', split_axis=0...  52.8 us
    all_to_all x1, waiting for transfers between devices, on_device(): lax.all_to_all(outgoing, 'ep', split_axis=0, concat_axis=0, tiled=True)  38.1 us
    all_gather x1, waiting for transfers between devices, on_device(): lax.all_gather(down_weight, 'tp', axis=1, tiled=True)  18.9 us
    ppermute x1, waiting for transfers between devices, padded_2(): lax.ppermute(tail, axis, [(i, (i + 1) % count) for i in range(ends)])  10.4 us
    dot_general x1, matrix products, expert_block_local(): first = jnp.dot(rows, gate, preferred_element_type=jnp.float32)  7.54 us
    dot_general x1, matrix products, expert_block_local(): second = jnp.dot(rows, upper, preferred_element_type=jnp.float32)  7.31 us
    all_to_all x1, starting transfers between devices, on_device(): lax.all_to_all(outgoing, 'ep', split_axis=0, concat_axis=0, tiled=True)  7.28 us
    gather x1, local copies, waits for them, and re-layouts, on_device(): pairs = answered[slots].reshape(local, 2, width)  7.03 us
  transfers between devices with their start and end apart: 8, of which 4 were waited for; matrix products, arithmetic and copies ran while one was open for 23% of the time, Pallas kernels for 0%

commit v1 on v0

--- a/solution.py
+++ b/solution.py
@@ -106,7 +106,9 @@
     whole_gate, whole_up, whole_down = (
         lax.all_gather(gate_weight, "tp", axis=2, tiled=True),
         lax.all_gather(up_weight, "tp", axis=2, tiled=True),
-        lax.all_gather(down_weight, "tp", axis=1, tiled=True),
+        jnp.concatenate(
+            lax.all_to_all(jnp.stack([down_weight] * lax.axis_size("tp")), "tp", 0, 0), axis=1
+        ),
     )
     arrived = lax.all_to_all(outgoing, "ep", split_axis=0, concat_axis=0, tiled=True)
     senders, items, _ = arrived.shape

time: 217 us -> 241 us (1.11)
  waiting for transfers between devices: 122 us -> 135 us
  matrix products: 28.8 us -> 32.4 us
  starting transfers between devices: 18.7 us -> 22 us
    all_to_all x0 -> x1, waiting for transfers between devices: none -> 21.1 us  [on_device(): lax.all_to_all(jnp.stack([down_weight] * lax.axis_size('tp')), 'tp', 0, 0)]
    all_gather x1 -> x0, waiting for transfers between devices: 18.9 us -> none  [on_device(): lax.all_gather(down_weight, 'tp', axis=1, tiled=True)]
    all_to_all x1, waiting for transfers between devices: 38.1 us -> 56.5 us  [on_device(): lax.all_to_all(outgoing, 'ep', split_axis=0, concat_axis=0, tiled=True)]
    ppermute x1, waiting for transfers between devices: 10.4 us -> 0.01 us  [padded_2(): lax.ppermute(tail, axis, [(i, (i + 1) % count) for i in range(ends)])]
    all_to_all x0 -> x1, starting transfers between devices: none -> 4.97 us  [on_device(): lax.all_to_all(jnp.stack([down_weight] * lax.axis_size('tp')), 'tp', 0, 0)]
    ppermute x1, waiting for transfers between devices: 0.01 us -> 3.95 us  [padded_2(): lax.ppermute(head, axis, [((i + 1) % count, i) for i in range(ends)])]
    another operation x0 -> x1, local copies, waits for them, and re-layouts: none -> 2.47 us  [on_device(): jnp.stack([down_weight] * lax.axis_size('tp'))]
where the time goes in v1:
time: 241 us; the launch traced here: 240 us
  waiting for transfers between devices  135 us (56%)
  matrix products  32.4 us (13%)
  local copies, waits for them, and re-layouts  23.6 us (10%)
  starting transfers between devices  22 us (9%)
  between operations  14.1 us (6%)
  other arithmetic  12.8 us (5%)
    all_to_all x1, waiting for transfers between devices, on_device(): lax.all_to_all(outgoing, 'ep', split_axis=0, concat_axis=0, tiled=True)  56.5 us
    all_to_all x1, waiting for transfers between devices, on_device(): lax.all_to_all(answers.reshape(senders, items, width), 'ep', split_axis=0...  52.2 us
    all_to_all x1, waiting for transfers between devices, on_device(): lax.all_to_all(jnp.stack([down_weight] * lax.axis_size('tp')), 'tp', 0, 0)  21.1 us
    dot_general x4, matrix products, blockwise_sum(): jnp.dot(left[:, block * width:(block + 1) * width], right[block * width:(...  8.3 us
    dot_general x1, matrix products, expert_block_local(): second = jnp.dot(rows, upper, preferred_element_type=jnp.float32)  7.37 us
    all_to_all x1, starting transfers between devices, on_device(): lax.all_to_all(outgoing, 'ep', split_axis=0, concat_axis=0, tiled=True)  7.28 us
    gather x1, local copies, waits for them, and re-layouts, on_device(): pairs = answered[slots].reshape(local, 2, width)  7.03 us
    dot_general x1, matrix products, expert_block_local(): first = jnp.dot(rows, gate, preferred_element_type=jnp.float32)  6.92 us
  transfers between devices with their start and end apart: 8, of which 4 were waited for; matrix products, arithmetic and copies ran while one was open for 23% of the time, Pallas kernels for 0%

profile of v1, /device:TPU:0, one launch (start us, length us, event | category | flops | bytes accessed | tf_op | source)
XLA Modules:
  0.0 240.1 jit_solution(1038259543088721644)
XLA Ops:
  7.2 0.0 copy-start
  7.2 0.0 all-gather.5.cloned.1.call-start
  7.2 0.7 all-gather.5.cloned.1.call-update
  7.9 0.8 copy.20
  8.7 0.1 eq.29
  8.9 0.9 reduce-window.6
  9.7 0.2 slice_reduce_fusion
  10.0 0.7 broadcast_multiply_fusion
  10.7 0.1 copy.19
  10.8 0.1 mul.158
  11.0 1.3 fusion.9
  12.3 1.3 fusion.11
  13.6 0.1 concatenate.7
  13.7 0.1 add_bitcast_fusion
  13.8 2.9 %scatter_custom_fusion = s32[640]{0:T(1024)S(1)} fusion(s32[320]{0:T(512)S(1)} %fusion.34, s32[320]{0:T(512)S(1)} %add_select_fusion, s32[]{:T(128)} %constant.59.clone.1), kind=kCustom, calls=%fused_computation.75 | custom fusion | bytes 2564 | tf_op jit(solution)/shard_map/scatter | solution.py:102
  16.7 4.1 %gather_fusion = bf16[640,2048]{1,0:T(8,128)(2,1)} fusion(bf16[161,2048]{1,0:T(8,128)(2,1)S(1)} %concatenate.7, s32[1024]{0:T(1024)S(1)} %pad_clamp_fusion.1), kind=kCustom, calls=%fused_computation | custom fusion | bytes 5245440 | tf_op jit(solution)/shard_map/gather | solution.py:105
  20.8 7.3 %all-to-all-start = ((bf16[8,80,2048]{2,1,0:T(8,128)(2,1)}), bf16[8,80,2048]{2,1,0:T(8,128)(2,1)}, u32[]{:S(2)}, u32[]{:S(2)}) async-start(bf16[8,80,2048]{2,1,0:T(8,128)(2,1)} %bitcast.54), calls=%async_computation.1 | async-start | bytes 5242880 | tf_op jit(solution)/shard_map/all_to_all | solution.py:113
  28.1 0.0 copy-start.2
  28.1 0.0 all-gather.3.cloned.1.call-start
  28.2 0.7 all-gather.3.cloned.1.call-update
  28.9 2.3 fusion
  31.2 56.5 %all-to-all-done = bf16[8,80,2048]{2,1,0:T(8,128)(2,1)} async-done(((bf16[8,80,2048]{2,1,0:T(8,128)(2,1)}), bf16[8,80,2048]{2,1,0:T(8,128)(2,1)}, u32[]{:S(2)}, u32[]{:S(2)}) %all-to-all-start) | async-done | bytes 2621472 | tf_op jit(solution)/shard_map/all_to_all | solution.py:113
  87.7 0.0 copy-done.2
  87.7 2.5 %stack.2 = bf16[4,1,256,2048]{3,2,1,0:T(8,128)(2,1)} broadcast(bf16[256,2048]{1,0:T(8,128)(2,1)S(1)} %bitcast.56), dimensions={2,3} | broadcast | bytes 5242880 | tf_op jit(solution)/shard_map/stack | solution.py:110
  90.1 0.0 copy-start.7
  90.2 5.0 %all-to-all-start.1 = ((bf16[4,1,256,2048]{3,2,1,0:T(8,128)(2,1)}), bf16[4,1,256,2048]{3,2,1,0:T(8,128)(2,1)}, u32[]{:S(2)}, u32[]{:S(2)}) async-start(bf16[4,1,256,2048]{3,2,1,0:T(8,128)(2,1)} %stack.2), calls=%async_computation.2 | async-start | bytes 8388608 | tf_op jit(solution)/shard_map/all_to_all | solution.py:110
  95.1 0.0 copy-done.7
  95.2 0.0 copy-done.10
  95.2 0.0 copy-start.1
  95.2 0.0 copy-start.8
  95.2 2.8 %fusion.37 = f32[640,256]{1,0:T(8,128)S(1)} fusion(bf16[2048,256]{1,0:T(8,128)(2,1)S(1)} %copy-done.7, bf16[640,2048]{1,0:T(8,128)(2,1)} %param.15, f32[2048]{0:T(1024)S(1)} %copy-done.10, f32[640]{0:T(1024)S(1)} %add_rsqrt_fusion), kind=kOutput, calls=%fused_computation.84 | convolution fusion | flops 676331520 | bytes 4336128 | tf_op jit(solution)/shard_map/dot_general | solution.py:75
  98.0 0.0 copy-done.1
  98.0 0.0 copy-done.8
  98.0 0.0 copy-start.5
  98.0 0.9 fusion.15
  99.0 3.4 %collective-permute-start = (bf16[1,256]{1,0:T(2,128)(2,1)S(1)}, bf16[1,256]{1,0:T(2,128)(2,1)S(1)}, u32[]{:S(2)}, u32[]{:S(2)}) collective-permute-start(bf16[1,256]{1,0:T(2,128)(2,1)S(1)} %get-tuple-element.4), channel_id=1, source_target_pairs={{0,4},{4,8},{8,12},{12,16},{16,20},{20,24},{24,28},{1,5},{5,9},{9,... | collective-permute-start | bytes 1544 | tf_op jit(solution)/shard_map/ppermute | solution.py:18
  102.3 1.5 collective-permute-start.1
  103.8 0.0 copy-done.5
  103.8 0.0 collective-permute-done
  103.9 4.0 %collective-permute-done.1 = bf16[1,256]{1,0:T(2,128)(2,1)S(1)} collective-permute-done((bf16[1,256]{1,0:T(2,128)(2,1)S(1)}, bf16[1,256]{1,0:T(2,128)(2,1)S(1)}, u32[]{:S(2)}, u32[]{:S(2)}) %collective-permute-start.1) | collective-permute-done | bytes 544 | tf_op jit(solution)/shard_map/ppermute | solution.py:20
  107.8 0.1 maximum_convert_fusion
  107.9 0.0 all-gather.5.cloned.1.call-done
  107.9 7.4 %fusion.3 = f32[640,1024]{1,0:T(8,128)} fusion(bf16[640,2048]{1,0:T(8,128)(2,1)} %bitcast.9, bf16[1,2048,1024]{2,1,0:T(8,128)(2,1)} %all-gather.5.cloned.1.call-done), kind=kOutput, calls=%fused_computation.9 | convolution fusion | flops 2684354560 | bytes 9437184 | tf_op jit(solution)/shard_map/dot_general | solution.py:132
  115.3 6.9 %multiply_convert_fusion = bf16[640,1024]{1,0:T(8,128)(2,1)S(1)} fusion(f32[640,1024]{1,0:T(8,128)} %fusion.3, bf16[640,2048]{1,0:T(8,128)(2,1)} %bitcast.9, bf16[1,2048,1024]{2,1,0:T(8,128)(2,1)} %all-gather.3.cloned.1.call-done), kind=kOutput, calls=%fused_computation.18 | convolution fusion | flops 2688286720 | bytes 10747904 | tf_op jit(solution)/shard_map/dot_general | solution.py:131
  122.2 21.1 %all-to-all-done.1 = bf16[4,1,256,2048]{3,2,1,0:T(8,128)(2,1)} async-done(((bf16[4,1,256,2048]{3,2,1,0:T(8,128)(2,1)}), bf16[4,1,256,2048]{3,2,1,0:T(8,128)(2,1)}, u32[]{:S(2)}, u32[]{:S(2)}) %all-to-all-start.1) | async-done | bytes 4194336 | tf_op jit(solution)/shard_map/all_to_all | solution.py:110
  143.3 2.1 convolution_convert_fusion.3
  145.4 2.1 convolution_convert_fusion.2
  147.5 2.1 convolution_convert_fusion.1
  149.6 2.1 convolution_convert_fusion
  151.7 3.8 %add_convert_fusion = bf16[640,2048]{1,0:T(8,128)(2,1)} fusion(bf16[640,2048]{1,0:T(8,128)(2,1)S(1)} %convolution_convert_fusion, bf16[640,2048]{1,0:T(8,128)(2,1)S(1)} %convolution_convert_fusion.1, bf16[640,2048]{1,0:T(8,128)(2,1)S(1)} %convolution_convert_fusion.2, bf16[640,2048]{1,0:T(8,128)(2,1)S(1)} %convolution_convert_fusion.3), kind=kLoop, calls=%fused_computation.8 | loop fusion | flops 10485760 | bytes 13107200 | tf_op jit(solution)/shard_map/convert_element_type | solution.py:44
  155.5 4.5 %all-to-all-start.2 = ((bf16[8,80,2048]{2,1,0:T(8,128)(2,1)}), bf16[8,80,2048]{2,1,0:T(8,128)(2,1)}, u32[]{:S(2)}, u32[]{:S(2)}) async-start(bf16[8,80,2048]{2,1,0:T(8,128)(2,1)} %bitcast.55), calls=%async_computation.3 | async-start | bytes 5242880 | tf_op jit(solution)/shard_map/all_to_all | solution.py:118
  160.0 0.3 reduce-scatter.2.cloned.1.call-start
  160.3 0.0 copy-done
  160.3 0.0 copy-done.9
  160.3 6.1 %convolution_convert_fusion.4 = bf16[640,2048]{1,0:T(8,128)(2,1)} fusion(bf16[256,2048]{1,0:T(8,128)(2,1)S(1)} %copy-done, bf16[2048,256]{1,0:T(8,128)(2,1)S(1)} %copy-done.9, f32[642,256]{1,0:T(8,128)S(1)} %maximum_convert_fusion, f32[256]{0:T(256)S(1)} %bitcast.62, f32[256]{0:T(256)S(1)} %bitcast.63, f32[256]{0:T(256)S(1)} %bitcast.61, ...), kind=kOutput, calls=%fused_computation.17 | convolution fusion | flops 1349877760 | bytes 9321472 | tf_op jit(solution)/shard_map/dot_general | solution.py:84
  166.5 0.0 reduce-scatter.2.cloned.1.call-update
  166.5 0.7 copy-done.4
  167.2 0.0 copy-done.3
  167.2 0.0 copy-done.6
  167.3 52.2 %all-to-all-done.2 = bf16[8,80,2048]{2,1,0:T(8,128)(2,1)} async-done(((bf16[8,80,2048]{2,1,0:T(8,128)(2,1)}), bf16[8,80,2048]{2,1,0:T(8,128)(2,1)}, u32[]{:S(2)}, u32[]{:S(2)}) %all-to-all-start.2) | async-done | bytes 2621472 | tf_op jit(solution)/shard_map/all_to_all | solution.py:118
  219.5 7.0 %gather_fusion.1 = bf16[320,2048]{1,0:T(8,128)(2,1)} fusion(bf16[640,2048]{1,0:T(8,128)(2,1)} %bitcast.18, s32[1024]{0:T(1024)S(1)} %pad_clamp_fusion), kind=kCustom, calls=%fused_computation.1 | custom fusion | bytes 2622720 | tf_op jit(solution)/shard_map/gather | solution.py:122
  226.5 3.1 %reshape.99 = bf16[160,2,2048]{2,1,0:T(2,128)(2,1)S(1)} reshape(bf16[320,2048]{1,0:T(8,128)(2,1)} %gather_fusion.1) | data formatting | bytes 2621440 | tf_op jit(solution)/shard_map/reshape | solution.py:122
  229.6 1.8 fusion.41
  231.4 2.2 fusion.13
  (24 shorter events, 0.2 us)
Async XLA Ops:
  7.2 153.2 %copy-start = (bf16[256,2048]{1,0:T(8,128)(2,1)S(1)}, bf16[256,2048]{1,0:T(8,128)(2,1)}, u32[]{:S(2)}) copy-start(bf16[256,2048]{1,0:T(8,128)(2,1)} %param.21) | copy-start | bytes 3145732
  7.2 100.7 %all-gather.5.cloned.1.call-start = ((), (), s32[]{:S(2)}) async-start(), calls=%async_computation.6 | async-start | bytes 5242880 | tf_op jit(solution)/shard_map/all_gather | solution.py:108
  20.8 66.9 %all-to-all-start = ((bf16[8,80,2048]{2,1,0:T(8,128)(2,1)}), bf16[8,80,2048]{2,1,0:T(8,128)(2,1)}, u32[]{:S(2)}, u32[]{:S(2)}) async-start(bf16[8,80,2048]{2,1,0:T(8,128)(2,1)} %bitcast.54), calls=%async_computation.1 | async-start | bytes 5242880 | tf_op jit(solution)/shard_map/all_to_all | solution.py:113
  28.1 59.6 %copy-start.2 = (bf16[1,256,2048]{2,1,0:T(8,128)(2,1)S(1)}, bf16[1,256,2048]{2,1,0:T(8,128)(2,1)}, u32[]{:S(2)}) copy-start(bf16[1,256,2048]{2,1,0:T(8,128)(2,1)} %param.29) | copy-start | bytes 3145732
  28.1 87.2 %all-gather.3.cloned.1.call-start = ((), (), s32[]{:S(2)}) async-start(), calls=%async_computation.5 | async-start | bytes 5242880 | tf_op jit(solution)/shard_map/all_gather | solution.py:107
  90.1 5.0 %copy-start.7 = (bf16[2048,256]{1,0:T(8,128)(2,1)S(1)}, bf16[2048,256]{1,0:T(8,128)(2,1)}, u32[]{:S(2)}) copy-start(bf16[2048,256]{1,0:T(8,128)(2,1)} %param.18) | copy-start | bytes 3145732
  90.2 5.0 %copy-start.10 = (f32[2048]{0:T(1024)S(1)}, f32[2048]{0:T(1024)}, u32[]{:S(2)}) copy-start(f32[2048]{0:T(1024)} %param.16) | copy-start | bytes 24580
  90.2 53.2 %all-to-all-start.1 = ((bf16[4,1,256,2048]{3,2,1,0:T(8,128)(2,1)}), bf16[4,1,256,2048]{3,2,1,0:T(8,128)(2,1)}, u32[]{:S(2)}, u32[]{:S(2)}) async-start(bf16[4,1,256,2048]{3,2,1,0:T(8,128)(2,1)} %stack.2), calls=%async_computation.2 | async-start | bytes 8388608 | tf_op jit(solution)/shard_map/all_to_all | solution.py:110
  95.2 2.8 %copy-start.1 = (bf16[640,2048]{1,0:T(8,128)(2,1)S(1)}, bf16[640,2048]{1,0:T(8,128)(2,1)}, u32[]{:S(2)}) copy-start(bf16[640,2048]{1,0:T(8,128)(2,1)} %param.15) | copy-start | bytes 7864324
  95.2 2.8 %copy-start.8 = (bf16[2048,256]{1,0:T(8,128)(2,1)S(1)}, bf16[2048,256]{1,0:T(8,128)(2,1)}, u32[]{:S(2)}) copy-start(bf16[2048,256]{1,0:T(8,128)(2,1)} %param.17) | copy-start | bytes 3145732
  98.0 5.8 %copy-start.5 = (f32[3,256]{1,0:T(4,128)S(1)}, f32[3,256]{1,0:T(4,128)}, u32[]{:S(2)}) copy-start(f32[3,256]{1,0:T(4,128)} %param.20) | copy-start | bytes 9220
  99.0 4.9 %collective-permute-start = (bf16[1,256]{1,0:T(2,128)(2,1)S(1)}, bf16[1,256]{1,0:T(2,128)(2,1)S(1)}, u32[]{:S(2)}, u32[]{:S(2)}) collective-permute-start(bf16[1,256]{1,0:T(2,128)(2,1)S(1)} %get-tuple-element.4), channel_id=1, source_target_pairs={{0,4},{4,8},{8,12},{12,16},{16,20},{20,24},{24,28},{1,5},{5,9},{9,... | collective-permute-start | bytes 1544 | tf_op jit(solution)/shard_map/ppermute | solution.py:18
  102.3 5.5 %collective-permute-start.1 = (bf16[1,256]{1,0:T(2,128)(2,1)S(1)}, bf16[1,256]{1,0:T(2,128)(2,1)S(1)}, u32[]{:S(2)}, u32[]{:S(2)}) collective-permute-start(bf16[1,256]{1,0:T(2,128)(2,1)S(1)} %get-tuple-element.5), channel_id=1, source_target_pairs={{4,0},{8,4},{12,8},{16,12},{20,16},{24,20},{28,24},{5,1},{9,5},{13... | collective-permute-start | bytes 1544 | tf_op jit(solution)/shard_map/ppermute | solution.py:20
  155.5 4.8 %copy-start.9 = (bf16[2048,256]{1,0:T(8,128)(2,1)S(1)}, bf16[2048,256]{1,0:T(8,128)(2,1)}, u32[]{:S(2)}) copy-start(bf16[2048,256]{1,0:T(8,128)(2,1)} %param.19) | copy-start | bytes 3145732
  155.5 64.0 %all-to-all-start.2 = ((bf16[8,80,2048]{2,1,0:T(8,128)(2,1)}), bf16[8,80,2048]{2,1,0:T(8,128)(2,1)}, u32[]{:S(2)}, u32[]{:S(2)}) async-start(bf16[8,80,2048]{2,1,0:T(8,128)(2,1)} %bitcast.55), calls=%async_computation.3 | async-start | bytes 5242880 | tf_op jit(solution)/shard_map/all_to_all | solution.py:118
  160.0 73.6 %reduce-scatter.2.cloned.1.call-start = ((), (), s32[]{:S(2)}) async-start(), calls=%async_computation.4 | async-start | bytes 3276800 | tf_op jit(solution)/shard_map/reduce_scatter | solution.py:83
  166.5 0.7 copy-start.4
  166.5 0.8 copy-start.3
  166.5 0.8 copy-start.6
Sparse Core Ops, SparseCore 0:
  9.5 37.7 all-gather.4
  48.8 34.9 all-gather.2
  166.6 34.6 reduce-scatter.1
